TPU v7x, 32 devices: a whole 2x2x4 slice. The times are simulated.
32 devices in a mesh: grp: 2 (over y), ep: 8 (over z, core), tp: 2 (over x).
Axes of the slice: x: 2, y: 2, z: 4, core: 2. Of those that a mesh axis runs over, the one named last changes fastest.
Arguments:
- recurrence_query_input: bfloat16 [2048, 2048], P(('grp', 'ep'), 'tp'), parts along dimension 0, may hold values from -6 to 6
- forget_gate_input: bfloat16 [2048, 2048], P(('grp', 'ep'), 'tp'), parts along dimension 0, may hold values from -6.5 to 6.5
- recurrence_value_input: bfloat16 [2048, 2048], P(('grp', 'ep'), 'tp'), parts along dimension 0, may hold values from -6 to 6
- output_gate_input: bfloat16 [2048, 2048], P(('grp', 'ep'), 'tp'), parts along dimension 0, may hold values from -6 to 6
- forget_lower_margin: float32 [2048], P('tp'), may hold values from 0 to 0.1
- position_decay_extra: float32 [2048, 16], P(('grp', 'ep'), 'tp'), parts along dimension 0, may hold values from -2.1 to 0
- head_norm_gain: float32 [2048], P('tp'), may hold values from 0.1 to 1.9
- recurrence_out_weight: bfloat16 [2048, 2048], P('tp'), may hold values from -0.125 to 0.125
- expert_hidden_state: bfloat16 [2048, 2048], P(('grp', 'ep')), parts along dimension 0, may hold values from -6 to 6
- chosen_expert_index: int32 [2048, 4], P(('grp', 'ep')), parts along dimension 0, may hold values from 0 to 7, all different within a row; in each aligned block of 128 rows (0 to 127, 128 to 255, ...) at most 128 rows name the same one
- chosen_expert_score: float32 [2048, 4], P(('grp', 'ep')), parts along dimension 0, may hold values from 0.02 to 1
- expert_norm_gain: float32 [2048], replicated, may hold values from 0.1 to 1.9
- routed_gate_weight: bfloat16 [8, 2048, 1024], P('ep', None, 'tp'), may hold values from -0.125 to 0.125
- routed_up_weight: bfloat16 [8, 2048, 1024], P('ep', None, 'tp'), may hold values from -0.125 to 0.125
- routed_down_weight: bfloat16 [8, 1024, 2048], P('ep', None, 'tp'), may hold values from -0.1875 to 0.1875
- shared_gate_weight: bfloat16 [2048, 1024], P(None, 'tp'), may hold values from -0.125 to 0.125
- shared_up_weight: bfloat16 [2048, 1024], P(None, 'tp'), may hold values from -0.125 to 0.125
- shared_down_weight: bfloat16 [1024, 2048], P(None, 'tp'), may hold values from -0.1875 to 0.1875
Outputs:
- recurrence_output: bfloat16 [2048, 2048], P(('grp', 'ep', 'tp')), parts along dimension 0
- expert_out: bfloat16 [2048, 2048], P(('grp', 'ep'), 'tp'), parts along dimension 0
There are 2 independent parts, one for each index of `grp`. A program takes and returns all parts, laid end to end along the dimension named above; an argument that names none is the same for every part. Nothing has to cross between parts.
Inputs may be any that keep to these rules, and one draw needn't show every extreme that they name: `chosen_expert_index`: each row names 4 different experts. In each aligned block of 128 rows (the rows of one index of ep) no expert is named by more than 128 rows, and in every draw some block names some expert exactly 128 times.
All inputs are finite; a program needn't handle non-finite values.
Results may differ from a plain program's by a relative error of at most 0.015.
Values may be sent and summed in bfloat16 or wider, within the bound.
A program may use at most 64 MiB of HBM per device.

v0:
```python
import jax
import jax.numpy as jnp
from jax import lax
from jax.sharding import PartitionSpec as P

HEAD_CHANNELS = 128
BLK = 64
EPSILON = 1e-06
ROUTED_SCALE = 2.5
PRECISION = lax.Precision.DEFAULT


def carried_in(array, axis, combine, identity):
    count, index = (lax.axis_size(axis), lax.axis_index(axis))
    everything = jax.tree.map(
        lambda part, kind: lax.all_gather(part.astype(kind), axis),
        array,
        (jnp.bfloat16, jnp.bfloat16),
    )
    start = jax.tree.map(
        lambda part, zero: jnp.broadcast_to(jnp.asarray(zero, part.dtype), part.shape),
        array,
        identity,
    )

    def turn(k, before):
        reached = k < index
        new = combine(
            before, jax.tree.map(lambda part, own: part[k].astype(own.dtype), everything, array)
        )
        return jax.tree.map(lambda a, b: jnp.where(reached, a, b), new, before)

    return lax.fori_loop(0, count, turn, start)


def chain_states(earlier, later):
    return (earlier[0] * later[0], later[0][..., None] * earlier[1] + later[1])


def mixer_half(
    recurrence_query_input,
    forget_gate_input,
    recurrence_value_input,
    output_gate_input,
    forget_lower_margin,
    position_decay_extra,
    head_norm_gain,
    recurrence_out_weight,
):
    length = recurrence_query_input.shape[0]
    head_tensor = position_decay_extra.shape[1]
    blocks = length // BLK
    queries = jax.nn.silu(recurrence_query_input.astype(jnp.float32))
    key_gate_value = forget_lower_margin[None, :] * jax.nn.sigmoid(
        -forget_gate_input.astype(jnp.float32)
    )
    decay_logarithm = jnp.log1p(-key_gate_value) + jnp.repeat(
        position_decay_extra, HEAD_CHANNELS, axis=1
    )
    value_rows = recurrence_value_input.astype(jnp.float32)

    def split_heads(tensor):
        return tensor.reshape(blocks, BLK, head_tensor, HEAD_CHANNELS).transpose(2, 0, 1, 3)

    query_heads = split_heads(queries)
    key_heads = split_heads(key_gate_value)
    value_heads = split_heads(value_rows)
    cum_decay = jnp.cumsum(split_heads(decay_logarithm), axis=2)
    middle = cum_decay[:, :, BLK // 2 - 1 : BLK // 2]
    block_end = cum_decay[:, :, BLK - 1 : BLK]
    scores = jnp.einsum(
        "hncd,hnsd->hncs",
        query_heads * jnp.exp(cum_decay - middle),
        key_heads * jnp.exp(middle - cum_decay),
        precision=PRECISION,
    )
    causal = jnp.tril(jnp.ones((BLK, BLK), dtype=bool))
    scores = jnp.where(causal, scores, 0.0)
    within = jnp.einsum("hncs,hnse->hnce", scores, value_heads, precision=PRECISION)
    updates = jnp.einsum(
        "hncd,hnce->nhde",
        key_heads * jnp.exp(block_end - cum_decay),
        value_heads,
        precision=PRECISION,
    )
    block_log = block_end[:, :, 0, :]
    block_decay = jnp.exp(block_log).transpose(1, 0, 2)

    def advance(carry_state, inputs):
        factor, update = inputs
        return (factor[..., None] * carry_state + update, carry_state)

    initial = jnp.zeros((head_tensor, HEAD_CHANNELS, HEAD_CHANNELS), jnp.float32)
    local_final, local_starts = lax.scan(advance, initial, (block_decay, updates))
    device_decay = jnp.exp(jnp.sum(block_log, axis=1))
    identity = (jnp.ones_like(device_decay), jnp.zeros_like(local_final))
    _, incoming = carried_in((device_decay, local_final), "ep", chain_states, identity)
    before = jnp.exp(jnp.cumsum(block_log, axis=1) - block_log).transpose(1, 0, 2)
    starts = local_starts + before[..., None] * incoming[None]
    carried = jnp.einsum(
        "hncd,nhde->hnce", query_heads * jnp.exp(cum_decay), starts, precision=PRECISION
    )
    outputs = (within + carried).transpose(1, 2, 0, 3).reshape(length, head_tensor, HEAD_CHANNELS)
    factor = lax.rsqrt(jnp.mean(outputs * outputs, axis=2, keepdims=True) + EPSILON)
    normed = (outputs * factor).reshape(length, head_tensor * HEAD_CHANNELS) * head_norm_gain[
        None, :
    ]
    gated_rows = (normed * jax.nn.silu(output_gate_input.astype(jnp.float32))).astype(jnp.bfloat16)
    return lax.psum_scatter(
        jnp.dot(gated_rows, recurrence_out_weight, preferred_element_type=jnp.float32).astype(
            jnp.bfloat16
        ),
        "tp",
        scatter_dimension=0,
        tiled=True,
    )


def expert_half(
    expert_hidden_state,
    chosen_expert_index,
    chosen_expert_score,
    expert_norm_gain,
    routed_gate_weight,
    routed_up_weight,
    routed_down_weight,
    shared_gate_weight,
    shared_up_weight,
    shared_down_weight,
):
    tokens, top = chosen_expert_index.shape
    local_experts = routed_gate_weight.shape[0]
    devices = lax.axis_size("ep")
    experts = local_experts * devices
    capacity = min(tokens, 2 * tokens * top // experts)
    width_out = routed_down_weight.shape[2]
    features = expert_hidden_state.astype(jnp.float32)
    normed = (
        features
        * lax.rsqrt(jnp.mean(features * features, axis=1, keepdims=True) + EPSILON)
        * expert_norm_gain[None, :]
    ).astype(jnp.bfloat16)
    gates = ROUTED_SCALE * chosen_expert_score / jnp.sum(chosen_expert_score, axis=1, keepdims=True)
    flat_ids = chosen_expert_index.reshape(-1)
    onehot = (flat_ids[:, None] == jnp.arange(experts, dtype=jnp.int32)[None, :]).astype(jnp.int32)
    places = jnp.sum(onehot * (jnp.cumsum(onehot, axis=0) - 1), axis=1)
    slots = flat_ids * capacity + places
    owners = (
        jnp.full((experts * capacity,), tokens, jnp.int32)
        .at[slots]
        .set(jnp.arange(tokens * top, dtype=jnp.int32) // top)
    )
    padded = jnp.concatenate([normed, jnp.zeros((1, normed.shape[1]), jnp.bfloat16)], axis=0)
    outgoing = padded[owners].reshape(experts, capacity, normed.shape[1])
    piece = lax.all_to_all(outgoing, "ep", split_axis=0, concat_axis=0, tiled=True)
    grouped = piece.reshape(devices, local_experts, piece.shape[1], piece.shape[2])
    gate_part = jnp.einsum(
        "secd,edh->sech", grouped, routed_gate_weight, preferred_element_type=jnp.float32
    )
    up_part = jnp.einsum(
        "secd,edh->sech", grouped, routed_up_weight, preferred_element_type=jnp.float32
    )
    hidden = (jax.nn.silu(gate_part) * up_part).astype(jnp.bfloat16)
    hidden_rows = hidden.reshape(devices * local_experts, piece.shape[1], hidden.shape[3])
    flat_hidden = hidden_rows.reshape(experts * capacity, hidden_rows.shape[2])
    shared_hidden = (
        jax.nn.silu(jnp.dot(normed, shared_gate_weight, preferred_element_type=jnp.float32))
        * jnp.dot(normed, shared_up_weight, preferred_element_type=jnp.float32)
    ).astype(jnp.bfloat16)
    start_values = (
        jnp.zeros((experts * capacity, width_out), jnp.float32),
        jnp.zeros((tokens, width_out), jnp.float32),
    )
    routed_piece = lax.all_gather(flat_hidden, "tp", axis=1, tiled=True)
    shared_piece = lax.all_gather(shared_hidden, "tp", axis=1, tiled=True)
    count = routed_piece.shape[1]
    grouped = routed_piece.reshape(devices, local_experts, capacity, count)
    routed = jnp.einsum(
        "secn,enk->seck", grouped, routed_down_weight, preferred_element_type=jnp.float32
    )
    shared = jnp.dot(shared_piece, shared_down_weight, preferred_element_type=jnp.float32)
    routed_sum = routed.reshape(start_values[0].shape)
    answers = routed_sum.astype(jnp.bfloat16).reshape(experts, capacity, width_out)
    returned = lax.all_to_all(answers, "ep", split_axis=0, concat_axis=0, tiled=True)
    picked_rows = returned.reshape(experts * capacity, width_out)[slots].reshape(
        tokens, top, width_out
    )
    combined = shared + jnp.sum(gates[:, :, None] * picked_rows.astype(jnp.float32), axis=1)
    return combined.astype(jnp.bfloat16)


def dense_expert_half(
    expert_hidden_state,
    chosen_expert_index,
    chosen_expert_score,
    expert_norm_gain,
    routed_gate_weight,
    routed_up_weight,
    routed_down_weight,
    shared_gate_weight,
    shared_up_weight,
    shared_down_weight,
):
    tokens, top = chosen_expert_index.shape
    experts = lax.axis_size("ep")
    features = expert_hidden_state.astype(jnp.float32)
    width = features.shape[1]
    normed = (
        features
        * lax.rsqrt(jnp.mean(features * features, axis=1, keepdims=True) + EPSILON)
        * expert_norm_gain[None, :]
    ).astype(jnp.bfloat16)
    gates = ROUTED_SCALE * chosen_expert_score / jnp.sum(chosen_expert_score, axis=1, keepdims=True)
    chosen = chosen_expert_index[:, :, None] == jnp.arange(64, dtype=jnp.int32)[None, None, :]
    gate_table = jnp.sum(jnp.where(chosen, gates[:, :, None], 0.0), axis=1)
    high = gate_table.astype(jnp.bfloat16)
    low = (gate_table - high.astype(jnp.float32)).astype(jnp.bfloat16)
    sent = jnp.concatenate([normed, high, low], axis=1)
    everything = lax.all_gather(sent, "ep", axis=0, tiled=True)
    rows = everything[:, :width]
    mine = jnp.arange(64, dtype=jnp.int32) == lax.axis_index("ep")
    tail = everything[:, width:].astype(jnp.float32)
    own_gate = jnp.sum(jnp.where(mine[None, :], tail[:, :64] + tail[:, 64:], 0.0), axis=1)
    shared_hidden = (
        jax.nn.silu(jnp.dot(normed, shared_gate_weight, preferred_element_type=jnp.float32))
        * jnp.dot(normed, shared_up_weight, preferred_element_type=jnp.float32)
    ).astype(jnp.bfloat16)
    gate_part = jnp.dot(rows, routed_gate_weight[0], preferred_element_type=jnp.float32)
    up_part = jnp.dot(rows, routed_up_weight[0], preferred_element_type=jnp.float32)
    hidden = (jax.nn.silu(gate_part) * up_part * own_gate[:, None]).astype(jnp.bfloat16)
    shared_full = lax.all_gather(shared_hidden, "tp", axis=1, tiled=True)
    hidden_full = lax.all_gather(hidden, "tp", axis=1, tiled=True)
    shared = jnp.dot(shared_full, shared_down_weight, preferred_element_type=jnp.float32)
    routed = jnp.dot(hidden_full, routed_down_weight[0], preferred_element_type=jnp.float32).astype(
        jnp.bfloat16
    )
    total = lax.psum_scatter(routed, "ep", scatter_dimension=0, tiled=True)
    return (shared + total.astype(jnp.float32)).astype(jnp.bfloat16)


def per_device(
    recurrence_query_input,
    forget_gate_input,
    recurrence_value_input,
    output_gate_input,
    forget_lower_margin,
    position_decay_extra,
    head_norm_gain,
    recurrence_out_weight,
    expert_hidden_state,
    chosen_expert_index,
    chosen_expert_score,
    expert_norm_gain,
    routed_gate_weight,
    routed_up_weight,
    routed_down_weight,
    shared_gate_weight,
    shared_up_weight,
    shared_down_weight,
):
    recurrence_output = mixer_half(
        recurrence_query_input,
        forget_gate_input,
        recurrence_value_input,
        output_gate_input,
        forget_lower_margin,
        position_decay_extra,
        head_norm_gain,
        recurrence_out_weight,
    )
    tokens, top = chosen_expert_index.shape
    experts = routed_gate_weight.shape[0] * lax.axis_size("ep")
    every_row_fits = 2 * top >= experts and routed_gate_weight.shape[0] == 1 and (experts <= 64)
    half = dense_expert_half if every_row_fits else expert_half
    expert_out = half(
        expert_hidden_state,
        chosen_expert_index,
        chosen_expert_score,
        expert_norm_gain,
        routed_gate_weight,
        routed_up_weight,
        routed_down_weight,
        shared_gate_weight,
        shared_up_weight,
        shared_down_weight,
    )
    return (recurrence_output, expert_out)


def solution(mesh):
    in_specs = (
        P(("grp", "ep"), "tp"),
        P(("grp", "ep"), "tp"),
        P(("grp", "ep"), "tp"),
        P(("grp", "ep"), "tp"),
        P("tp"),
        P(("grp", "ep"), "tp"),
        P("tp"),
        P("tp", None),
        P(("grp", "ep"), None),
        P(("grp", "ep"), None),
        P(("grp", "ep"), None),
        P(),
        P("ep", None, "tp"),
        P("ep", None, "tp"),
        P("ep", None, "tp"),
        P(None, "tp"),
        P(None, "tp"),
        P(None, "tp"),
    )
    out_specs = (P(("grp", "ep", "tp"), None), P(("grp", "ep"), "tp"))
    return jax.shard_map(
        per_device, mesh=mesh, in_specs=in_specs, out_specs=out_specs, check_vma=False
    )
```

profile of v0, /device:TPU:0, one launch (start us, length us, event | category | flops | bytes accessed | tf_op | source)
XLA Modules:
  0.0 198.3 jit_solution(6184943672864648955)
XLA Ops:
  7.3 1.4 fusion.22
  16.9 1.9 fusion.38
  18.8 46.3 %all-gather.6.cloned.1.call-done = bf16[1024,2176]{1,0:T(8,128)(2,1)} async-done(((bf16[128,2176]{1,0:T(8,128)(2,1)}), bf16[1024,2176]{1,0:T(8,128)(2,1)}) %all-gather.6.cloned.1.call-update) | async-done | bytes 4456464 | tf_op jit(solution)/shard_map/all_gather | solution.py:219
  66.5 5.3 %fusion.3 = f32[1024,512]{1,0:T(8,128)S(1)} fusion(bf16[1024,2176]{1,0:T(8,128)(2,1)} %all-gather.6.cloned.1.call-done, bf16[1,2048,512]{2,1,0:T(8,128)(2,1)} %param.34), kind=kOutput, calls=%fused_computation.8 | convolution fusion | flops 2147483648 | bytes 8388608 | tf_op jit(solution)/shard_map/dot_general | solution.py:228
  71.9 3.6 %multiply_convert_fusion = bf16[1024,512]{1,0:T(8,128)(2,1)} fusion(f32[1024,512]{1,0:T(8,128)S(1)} %fusion.3, bf16[1,2048,512]{2,1,0:T(8,128)(2,1)S(1)} %copy-done.8, bf16[1024,2176]{1,0:T(8,128)(2,1)S(1)} %bitcast.139, f32[1024]{0:T(1024)S(1)} %fusion.37), kind=kOutput, calls=%fused_computation.15 | convolution fusion | flops 2151153664 | bytes 9441280 | tf_op jit(solution)/shard_map/dot_general | solution.py:229
  77.0 2.5 %bitcast_multiply_fusion.1 = (bf16[8,2,64,128]{3,0,1,2:T(8,128)(2,1)S(1)}, bf16[8,2,64,128]{3,0,1,2:T(8,128)(2,1)}, bf16[8,2,64,128]{3,0,1,2:T(8,128)(2,1)}, bf16[8,2,64,128]{3,0,1,2:T(8,128)(2,1)}) fusion(f32[8,2,64,128]{3,0,1,2:T(8,128)} %fusion.38, f32[8,2,128]{2,0,1:T(8,128)S(1)} %get-tuple-element.192, f32[8,2,128]{2,0,1:T(8,128)S(1)} %get-tuple-element.193, ...), kind=kLoop, calls=%fused_computation.54 | loop fusion | flops 1441792 | bytes 2637824 | tf_op jit(solution)/shard_map/mul | solution.py:82
  79.5 1.3 fusion.41
  80.8 4.5 %while.27 = (s32[]{:T(128)}, f32[8,128,128]{2,1,0:T(8,128)S(1)}, f32[2,8,128,128]{3,2,1,0:T(8,128)}, f32[2,8,128]{2,1,0:T(8,128)S(1)}, f32[2,8,128,128]{3,2,1,0:T(8,128)}, /*index=5*/s32[]{:T(128)}, s32[]{:T(128)}) while((s32[]{:T(128)}, f32[8,128,128]{2,1,0:T(8,128)S(1)}, f32[2,8,128,128]{3,2,1,0:T(8,128)}, ...), condition=%wide.region_2.3_spmd.clone, body=%wide.region_1.2_spmd.clone.sunk | while | flops 524291 | bytes 2633836 | solution.py:94
  81.7 1.4 bitcast_add_fusion.3
  83.9 1.4 bitcast_add_fusion.3
  86.2 12.8 %all-gather = bf16[64,128]{1,0:T(8,128)(2,1)S(1)} all-gather(bf16[8,128]{1,0:T(8,128)(2,1)S(1)} %exponential_convert_fusion), channel_id=2, replica_groups=mesh['grp'=2,'ep'=8,'tp'=2] {'ep'}, dimensions={0}, use_global_device_ids=true | all-gather | bytes 18432 | tf_op jit(solution)/shard_map/all_gather | solution.py:16
  100.5 7.1 %all-gather.8.cloned.1.call-done = bf16[1024,1024]{1,0:T(8,128)(2,1)} async-done(((bf16[1024,512]{1,0:T(8,128)(2,1)}), bf16[1024,1024]{1,0:T(8,128)(2,1)}) %all-gather.8.cloned.1.call-update) | async-done | bytes 2097168 | tf_op jit(solution)/shard_map/all_gather | solution.py:232
  107.6 5.2 %fusion.9 = bf16[1024,1024]{1,0:T(8,128)(2,1)} fusion(bf16[1024,1024]{1,0:T(8,128)(2,1)} %all-gather.8.cloned.1.call-done, bf16[1,1024,1024]{2,1,0:T(8,128)(2,1)S(1)} %copy-done), kind=kOutput, calls=%fused_computation.16 | convolution fusion | flops 2148532224 | bytes 6291456 | tf_op jit(solution)/shard_map/dot_general | solution.py:234
  113.7 2.2 %fusion.17 = f32[8,2,64,128]{3,2,1,0:T(8,128)} fusion(bf16[8,2,64,128]{3,0,1,2:T(8,128)(2,1)S(1)} %copy-done.4, bf16[8,2,64,128]{3,0,1,2:T(8,128)(2,1)} %get-tuple-element.189, bf16[8,2,64,128]{3,0,2,1:T(8,128)(2,1)} %bitcast_bitcast_fusion, pred[64,64]{1,0:T(8,128)(4,1)S(1)} %iota_compare_fusion.1), kind=kOutput, calls=%fused_computation.22 | convolution fusion | flops 33619968 | bytes 1314816 | tf_op jit(solution)/shard_map/hncs,hnse->hnce/dot_general | solution.py:79
  115.9 22.4 %all-gather.10.cloned.1.call-done = bf16[64,128,128]{2,1,0:T(8,128)(2,1)} async-done(((bf16[8,128,128]{2,1,0:T(8,128)(2,1)}), bf16[64,128,128]{2,1,0:T(8,128)(2,1)}) %all-gather.10.cloned.1.call-update) | async-done | bytes 2097168 | tf_op jit(solution)/shard_map/all_gather | solution.py:16
  138.3 10.8 %while.28 = (s32[]{:T(128)}, f32[8,128,128]{2,1,0:T(8,128)S(1)}, s32[]{:T(128)}, bf16[8,8,128]{2,1,0:T(8,128)(2,1)S(1)}, bf16[8,8,128,128]{3,2,1,0:T(8,128)(2,1)}, /*index=5*/s32[]{:T(128)}, s32[]{:T(128)}) while((s32[]{:T(128)}, f32[8,128,128]{2,1,0:T(8,128)S(1)}, s32[]{:T(128)}, bf16[8,8,128]{2,1,0:T(8,128)(2,1)S(1)}, ...), condition=%wide.region_6.7_spmd.clone, body=%wide.region_5.6_spmd.clone.sunk | while | flops 656388 | bytes 1321073 | solution.py:33
  149.2 2.7 %multiply_reduce_fusion = (f32[2,64,8]{1,0,2:T(2,128)S(1)}, f32[2,64,8,128]{3,1,0,2:T(8,128)}) fusion(f32[8,2,64,128]{3,2,1,0:T(8,128)} %fusion.17, bf16[8,2,64,128]{3,0,1,2:T(8,128)(2,1)S(1)} %copy-done.1, f32[2,8,128,128]{3,2,1,0:T(8,128)} %get-tuple-element.124, f32[8,128,128]{2,1,0:T(8,128)S(1)} %get-tuple-element.126, f32[2,8,128]{2,1,0:T(8,128)S(1)} %fusion.21), kind=kOutput, calls=%fused_computation.66 | convolution fusion | flops 34733056 | bytes 2895872 | tf_op jit(solution)/shard_map/hncd,nhde->hnce/dot_general | solution.py:100
  151.9 1.4 copy.67
  153.5 4.0 %convolution_convert_fusion = bf16[128,2048]{1,0:T(8,128)(2,1)} fusion(bf16[1024,2048]{1,0:T(8,128)(2,1)} %param.29, bf16[128,1024]{1,0:T(8,128)(2,1)} %param.25, f32[16,8,8,128]{3,2,1,0:T(8,128)S(1)} %bitcast.133, f32[16,8,8,128]{3,2,1,0:T(8,128)S(1)} %bitcast.134, f32[1024]{0:T(1024)S(1)} %copy-done.10), kind=kOutput, calls=%fused_computation.10 | convolution fusion | flops 538312704 | bytes 6033408 | tf_op jit(solution)/shard_map/dot_general | solution.py:110
  157.6 2.2 %fusion.60 = f32[128,512]{1,0:T(8,128)S(1)} fusion(bf16[128,2048]{1,0:T(8,128)(2,1)S(1)} %fusion.24, bf16[2048,512]{1,0:T(8,128)(2,1)} %param.37), kind=kOutput, calls=%fused_computation.94 | convolution fusion | flops 268435456 | bytes 2883584 | tf_op jit(solution)/shard_map/dot_general | solution.py:225
  160.3 6.3 %all_gather.22 = bf16[128,1024]{1,0:T(8,128)(2,1)S(1)} all-gather(bf16[128,512]{1,0:T(8,128)(2,1)S(1)} %fusion.19), channel_id=1, replica_groups=mesh['grp'=2,'ep'=8,'tp'=2] {'tp'}, dimensions={1}, use_global_device_ids=true | all-gather | bytes 393216 | tf_op jit(solution)/shard_map/all_gather | solution.py:231
  166.6 9.4 %reduce-scatter.5.cloned.1.call-done = bf16[128,1024]{1,0:T(8,128)(2,1)} async-done(((bf16[1024,1024]{1,0:T(8,128)(2,1)}), bf16[128,1024]{1,0:T(8,128)(2,1)}) %reduce-scatter.5.cloned.1.call-update) | async-done | bytes 262160 | tf_op jit(solution)/shard_map/reduce_scatter | solution.py:237
  176.0 2.7 %fusion.18 = bf16[128,1024]{1,0:T(8,128)(2,1)} fusion(bf16[128,1024]{1,0:T(8,128)(2,1)S(1)} %all_gather.22, bf16[1024,1024]{1,0:T(8,128)(2,1)} %param.39, bf16[128,1024]{1,0:T(8,128)(2,1)} %reduce-scatter.5.cloned.1.call-done), kind=kOutput, calls=%fused_computation.24 | convolution fusion | flops 268828672 | bytes 2883584 | tf_op jit(solution)/shard_map/dot_general | solution.py:233
  178.7 13.0 %reduce-scatter.3.cloned.1.call-done = bf16[64,2048]{1,0:T(8,128)(2,1)} async-done(((bf16[128,2048]{1,0:T(8,128)(2,1)}), bf16[64,2048]{1,0:T(8,128)(2,1)}) %reduce-scatter.3.cloned.1.call-update) | async-done | bytes 262160 | tf_op jit(solution)/shard_map/reduce_scatter | solution.py:109
  (91 shorter events, 27.4 us)
Async XLA Ops:
  7.2 100.4 %copy-start = (bf16[1,1024,1024]{2,1,0:T(8,128)(2,1)S(1)}, bf16[1,1024,1024]{2,1,0:T(8,128)(2,1)}, u32[]{:S(2)}) copy-start(bf16[1,1024,1024]{2,1,0:T(8,128)(2,1)} %param.36) | copy-start | bytes 6291460
  7.2 6.1 %copy-start.7 = (f32[128,8]{0,1:T(8,128)S(1)}, f32[128,8]{0,1:T(8,128)}, u32[]{:S(2)}) copy-start(f32[128,8]{0,1:T(8,128)} %param.27) | copy-start | bytes 12292
  7.2 6.4 %copy-start.2 = (bf16[128,1024]{1,0:T(8,128)(2,1)S(1)}, bf16[128,1024]{1,0:T(8,128)(2,1)}, u32[]{:S(2)}) copy-start(bf16[128,1024]{1,0:T(8,128)(2,1)} %param.23) | copy-start | bytes 786436
  7.2 6.4 %copy-start.6 = (f32[1024]{0:T(1024)S(1)}, f32[1024]{0:T(1024)}, u32[]{:S(2)}) copy-start(f32[1024]{0:T(1024)} %param.26) | copy-start | bytes 12292
  7.2 57.9 %all-gather.6.cloned.1.call-start = ((), (), s32[]{:S(2)}) async-start(), calls=%async_computation.3 | async-start | bytes 5013504 | tf_op jit(solution)/shard_map/all_gather | solution.py:219
  13.2 94.3 %all-gather.8.cloned.1.call-start = ((), (), s32[]{:S(2)}) async-start(), calls=%async_computation.4 | async-start | bytes 3145728 | tf_op jit(solution)/shard_map/all_gather | solution.py:232
  13.4 1.5 copy-start.3
  14.0 2.9 %copy-start.5 = (bf16[128,1024]{1,0:T(8,128)(2,1)S(1)}, bf16[128,1024]{1,0:T(8,128)(2,1)}, u32[]{:S(2)}) copy-start(bf16[128,1024]{1,0:T(8,128)(2,1)} %param.24) | copy-start | bytes 786436
  66.1 5.8 %slice-start = ((s8[4456448]{0:T(1024)(128)(4,1)}), s8[4194304]{0:T(1024)(128)(4,1)S(1)}, s32[]{:S(2)}) async-start(s8[4456448]{0:T(1024)(128)(4,1)} %bitcast.138), calls=%async_computation.7 | async-start | bytes 8388608
  66.5 5.4 %slice-start.1 = ((s8[4456448]{0:T(1024)(128)(4,1)}), s8[262144]{0:T(1024)(128)(4,1)S(1)}, s32[]{:S(2)}) async-start(s8[4456448]{0:T(1024)(128)(4,1)} %bitcast.138), calls=%async_computation.8 | async-start | bytes 524288
  66.5 5.4 %copy-start.8 = (bf16[1,2048,512]{2,1,0:T(8,128)(2,1)S(1)}, bf16[1,2048,512]{2,1,0:T(8,128)(2,1)}, u32[]{:S(2)}) copy-start(bf16[1,2048,512]{2,1,0:T(8,128)(2,1)} %param.35) | copy-start | bytes 6291460
  75.5 62.8 %all-gather.10.cloned.1.call-start = ((), (), s32[]{:S(2)}) async-start(), calls=%async_computation.6 | async-start | bytes 2359296 | tf_op jit(solution)/shard_map/all_gather | solution.py:16
  86.1 89.9 %reduce-scatter.5.cloned.1.call-start = ((), (), s32[]{:S(2)}) async-start(), calls=%async_computation.5 | async-start | bytes 2359296 | tf_op jit(solution)/shard_map/reduce_scatter | solution.py:237
  112.8 0.9 copy-start.4
  112.8 79.0 %reduce-scatter.3.cloned.1.call-start = ((), (), s32[]{:S(2)}) async-start(), calls=%async_computation.2 | async-start | bytes 786432 | tf_op jit(solution)/shard_map/reduce_scatter | solution.py:109
  138.3 10.8 %copy-start.1 = (bf16[8,2,64,128]{3,0,1,2:T(8,128)(2,1)S(1)}, bf16[8,2,64,128]{3,0,1,2:T(8,128)(2,1)}, u32[]{:S(2)}) copy-start(bf16[8,2,64,128]{3,0,1,2:T(8,128)(2,1)} %get-tuple-element.190) | copy-start | bytes 786436
  149.1 4.3 %copy-start.10 = (f32[1024]{0:T(1024)S(1)}, f32[1024]{0:T(1024)}, u32[]{:S(2)}) copy-start(f32[1024]{0:T(1024)} %param.28) | copy-start | bytes 12292
  157.5 2.3 %copy-start.9 = (bf16[2048,512]{1,0:T(8,128)(2,1)S(1)}, bf16[2048,512]{1,0:T(8,128)(2,1)}, u32[]{:S(2)}) copy-start(bf16[2048,512]{1,0:T(8,128)(2,1)} %param.38) | copy-start | bytes 6291460
Sparse Core Ops, SparseCore 0:
  13.4 51.7 all-gather.5
  75.6 31.8 all-gather.7
  109.2 29.1 all-gather.9
  140.5 35.4 reduce-scatter.4
  178.7 13.0 reduce-scatter.2
where the time goes:
time: 199 us; the launch traced here: 198 us
  waiting for transfers between devices  98.3 us (49%)
  matrix products  29.8 us (15%)
  other arithmetic  28.2 us (14%)
  blocking collectives  19.1 us (10%)
  between operations  14.1 us (7%)
  local copies, waits for them, and re-layouts  8.28 us (4%)
    all_gather x1, waiting for transfers between devices, dense_expert_half(): everything = lax.all_gather(sent, 'ep', axis=0, tiled=True)  46.3 us
    all_gather x1, waiting for transfers between devices, carried_in(): lax.all_gather(part.astype(kind), axis)  22.4 us
    reduce_scatter x1, waiting for transfers between devices, mixer_half(): lax.psum_scatter(jnp.dot(gated_rows, recurrence_out_weight, preferred_ele...  13 us
    all_gather x1, blocking collectives, carried_in(): lax.all_gather(part.astype(kind), axis)  12.8 us
    select_n x8, other arithmetic, turn(): return jax.tree.map(lambda a, b: jnp.where(reached, a, b), new, before)  10.4 us
    reduce_scatter x1, waiting for transfers between devices, dense_expert_half(): total = lax.psum_scatter(routed, 'ep', scatter_dimension=0, tiled=True)  9.4 us
    all_gather x1, waiting for transfers between devices, dense_expert_half(): hidden_full = lax.all_gather(hidden, 'tp', axis=1, tiled=True)  7.09 us
    all_gather x1, blocking collectives, dense_expert_half(): shared_full = lax.all_gather(shared_hidden, 'tp', axis=1, tiled=True)  6.33 us
  transfers between devices with their start and end apart: 5, of which 5 were waited for; matrix products, arithmetic and copies ran while one was open for 25% of the time, Pallas kernels for 0%

commit v1 on v0

--- a/solution.py
+++ b/solution.py
@@ -8,6 +8,17 @@
 EPSILON = 1e-06
 ROUTED_SCALE = 2.5
 PRECISION = lax.Precision.DEFAULT
+
+
+def around_the_ring(value, axis, d):
+    size = lax.axis_size(axis)
+    right = [(i, (i + 1) % size) for i in range(size)]
+    shards = [value]
+    for stride in range(1, size):
+        shards = [lax.ppermute(shards[0], axis, right), *shards]
+    full = jnp.concatenate(shards, axis=d)
+    places = (lax.axis_index(axis) + 1) * shards[-1].shape[d]
+    return jnp.roll(full, places, axis=d)
 
 
 def carried_in(array, axis, combine, identity):
@@ -216,7 +227,7 @@
     high = gate_table.astype(jnp.bfloat16)
     low = (gate_table - high.astype(jnp.float32)).astype(jnp.bfloat16)
     sent = jnp.concatenate([normed, high, low], axis=1)
-    everything = lax.all_gather(sent, "ep", axis=0, tiled=True)
+    everything = around_the_ring(sent, "ep", 0)
     rows = everything[:, :width]
     mine = jnp.arange(64, dtype=jnp.int32) == lax.axis_index("ep")
     tail = everything[:, width:].astype(jnp.float32)

time: 199 us -> 231 us (1.16)
  waiting for transfers between devices: 98.3 us -> 125 us
  local copies, waits for them, and re-layouts: 8.28 us -> 16.3 us
    ppermute x0 -> x7, waiting for transfers between devices: none -> 69.1 us  [around_the_ring(): shards = [lax.ppermute(shards[0], axis, right), *shards]]
    all_gather x1 -> x0, waiting for transfers between devices: 46.3 us -> none  [dense_expert_half(): everything = lax.all_gather(sent, 'ep', axis=0, tiled=True)]
    unnamed x31 -> x60, local copies, waits for them, and re-layouts: 3.83 us -> 14.2 us
    dot_general x1, matrix products: 5.35 us -> 2.32 us  [dense_expert_half(): jnp.dot(rows, routed_gate_weight[0], preferred_element_type=jnp.float32)]
  transfers between devices with their start and end apart: 5 -> 11, of which waited for: 5 -> 11; matrix products, arithmetic and copies ran while one was open for 25% -> 21% of each run, Pallas kernels for 0% -> 0%
where the time goes in v1:
time: 231 us; the launch traced here: 230 us
  waiting for transfers between devices  125 us (54%)
  matrix products  27.5 us (12%)
  other arithmetic  26.7 us (12%)
  blocking collectives  19.1 us (8%)
  local copies, waits for them, and re-layouts  16.3 us (7%)
  between operations  14.3 us (6%)
    ppermute x7, waiting for transfers between devices, around_the_ring(): shards = [lax.ppermute(shards[0], axis, right), *shards]  69.1 us
    all_gather x1, waiting for transfers between devices, carried_in(): lax.all_gather(part.astype(kind), axis)  23.1 us
    unnamed x60, local copies, waits for them, and re-layouts  14.2 us
    reduce_scatter x1, waiting for transfers between devices, mixer_half(): lax.psum_scatter(jnp.dot(gated_rows, recurrence_out_weight, preferred_ele...  13.3 us
    all_gather x1, blocking collectives, carried_in(): lax.all_gather(part.astype(kind), axis)  12.8 us
    select_n x8, other arithmetic, turn(): return jax.tree.map(lambda a, b: jnp.where(reached, a, b), new, before)  10.4 us
    reduce_scatter x1, waiting for transfers between devices, dense_expert_half(): total = lax.psum_scatter(routed, 'ep', scatter_dimension=0, tiled=True)  9.76 us
    all_gather x1, waiting for transfers between devices, dense_expert_half(): hidden_full = lax.all_gather(hidden, 'tp', axis=1, tiled=True)  9.3 us
  transfers between devices with their start and end apart: 11, of which 11 were waited for; matrix products, arithmetic and copies ran while one was open for 21% of the time, Pallas kernels for 0%

profile of v1, /device:TPU:0, one launch (start us, length us, event | category | flops | bytes accessed | tf_op | source)
XLA Modules:
  0.0 229.7 jit_solution(13747886686071996286)
XLA Ops:
  13.1 11.2 %collective-permute-done = bf16[128,2176]{1,0:T(8,128)(2,1)S(1)} collective-permute-done((bf16[128,2176]{1,0:T(8,128)(2,1)S(1)}, bf16[128,2176]{1,0:T(8,128)(2,1)S(1)}, u32[]{:S(2)}, u32[]{:S(2)}) %collective-permute-start) | collective-permute-done | bytes 557088 | tf_op jit(solution)/shard_map/ppermute | solution.py:18
  25.1 10.8 %collective-permute-done.1 = bf16[128,2176]{1,0:T(8,128)(2,1)S(1)} collective-permute-done((bf16[128,2176]{1,0:T(8,128)(2,1)S(1)}, bf16[128,2176]{1,0:T(8,128)(2,1)S(1)}, u32[]{:S(2)}, u32[]{:S(2)}) %collective-permute-start.1) | collective-permute-done | bytes 557088 | tf_op jit(solution)/shard_map/ppermute | solution.py:18
  36.7 10.8 %collective-permute-done.2 = bf16[128,2176]{1,0:T(8,128)(2,1)S(1)} collective-permute-done((bf16[128,2176]{1,0:T(8,128)(2,1)S(1)}, bf16[128,2176]{1,0:T(8,128)(2,1)S(1)}, u32[]{:S(2)}, u32[]{:S(2)}) %collective-permute-start.2) | collective-permute-done | bytes 557088 | tf_op jit(solution)/shard_map/ppermute | solution.py:18
  48.3 10.8 %collective-permute-done.3 = bf16[128,2176]{1,0:T(8,128)(2,1)S(1)} collective-permute-done((bf16[128,2176]{1,0:T(8,128)(2,1)S(1)}, bf16[128,2176]{1,0:T(8,128)(2,1)S(1)}, u32[]{:S(2)}, u32[]{:S(2)}) %collective-permute-start.3) | collective-permute-done | bytes 557088 | tf_op jit(solution)/shard_map/ppermute | solution.py:18
  59.8 10.9 %collective-permute-done.4 = bf16[128,2176]{1,0:T(8,128)(2,1)} collective-permute-done((bf16[128,2176]{1,0:T(8,128)(2,1)S(1)}, bf16[128,2176]{1,0:T(8,128)(2,1)}, u32[]{:S(2)}, u32[]{:S(2)}) %collective-permute-start.4) | collective-permute-done | bytes 557088 | tf_op jit(solution)/shard_map/ppermute | solution.py:18
  74.8 7.0 %collective-permute-done.5 = bf16[128,2176]{1,0:T(8,128)(2,1)} collective-permute-done((bf16[128,2176]{1,0:T(8,128)(2,1)}, bf16[128,2176]{1,0:T(8,128)(2,1)}, u32[]{:S(2)}, u32[]{:S(2)}) %collective-permute-start.5) | collective-permute-done | bytes 557088 | tf_op jit(solution)/shard_map/ppermute | solution.py:18
  83.0 2.1 fusion.34
  85.0 7.8 %collective-permute-done.6 = bf16[128,2176]{1,0:T(8,128)(2,1)} collective-permute-done((bf16[128,2176]{1,0:T(8,128)(2,1)}, bf16[128,2176]{1,0:T(8,128)(2,1)}, u32[]{:S(2)}, u32[]{:S(2)}) %collective-permute-start.6) | collective-permute-done | bytes 557088 | tf_op jit(solution)/shard_map/ppermute | solution.py:18
  100.4 2.3 %fusion.3 = f32[1024,512]{1,0:T(8,128)S(1)} fusion(bf16[2048,2176]{1,0:T(8,128)(2,1)S(1)} %constant_dynamic-update-slice_fusion, s32[]{:T(128)S(6)} %select_n.52, bf16[1,2048,512]{2,1,0:T(8,128)(2,1)S(1)} %copy-done.17), kind=kOutput, calls=%fused_computation.8 | convolution fusion | flops 2147483648 | bytes 8388612 | tf_op jit(solution)/shard_map/dot_general | solution.py:239
  103.1 3.6 %multiply_convert_fusion = bf16[1024,512]{1,0:T(8,128)(2,1)} fusion(f32[1024,512]{1,0:T(8,128)S(1)} %fusion.3, f32[1024]{0:T(1024)S(1)} %fusion.33, bf16[1,2048,512]{2,1,0:T(8,128)(2,1)S(1)} %copy-done.18, bf16[2048,2176]{1,0:T(8,128)(2,1)S(1)} %constant_dynamic-update-slice_fusion, s32[]{:T(128)S(6)} %select_n.52), kind=kOutput, calls=%fused_computation.15 | convolution fusion | flops 2151153664 | bytes 9441284 | tf_op jit(solution)/shard_map/dot_general | solution.py:240
  106.8 2.3 %bitcast_multiply_fusion.1 = (bf16[8,2,64,128]{3,0,1,2:T(8,128)(2,1)S(1)}, bf16[8,2,64,128]{3,0,1,2:T(8,128)(2,1)}, bf16[8,2,64,128]{3,0,1,2:T(8,128)(2,1)}, bf16[8,2,64,128]{3,0,1,2:T(8,128)(2,1)}) fusion(f32[8,2,64,128]{3,0,1,2:T(8,128)S(1)} %copy-done.3, f32[8,2,128]{2,0,1:T(8,128)S(1)} %get-tuple-element.192, f32[8,2,128]{2,0,1:T(8,128)S(1)} %get-tuple-element.193, ...), kind=kLoop, calls=%fused_computation.54 | loop fusion | flops 1441792 | bytes 2637824 | tf_op jit(solution)/shard_map/mul | solution.py:93
  110.5 4.4 %while.27 = (s32[]{:T(128)}, f32[8,128,128]{2,1,0:T(8,128)S(1)}, f32[2,8,128,128]{3,2,1,0:T(8,128)}, f32[2,8,128]{2,1,0:T(8,128)S(1)}, f32[2,8,128,128]{3,2,1,0:T(8,128)}, /*index=5*/s32[]{:T(128)}, s32[]{:T(128)}) while((s32[]{:T(128)}, f32[8,128,128]{2,1,0:T(8,128)S(1)}, f32[2,8,128,128]{3,2,1,0:T(8,128)}, ...), condition=%wide.region_2.3_spmd.clone, body=%wide.region_1.2_spmd.clone.sunk | while | flops 524291 | bytes 2634336 | solution.py:105
  115.8 12.8 %all-gather = bf16[64,128]{1,0:T(8,128)(2,1)S(1)} all-gather(bf16[8,128]{1,0:T(8,128)(2,1)S(1)} %exponential_convert_fusion), channel_id=2, replica_groups=mesh['grp'=2,'ep'=8,'tp'=2] {'ep'}, dimensions={0}, use_global_device_ids=true | all-gather | bytes 18432 | tf_op jit(solution)/shard_map/all_gather | solution.py:27
  129.4 9.3 %all-gather.5.cloned.1.call-done = bf16[1024,1024]{1,0:T(8,128)(2,1)} async-done(((bf16[1024,512]{1,0:T(8,128)(2,1)}), bf16[1024,1024]{1,0:T(8,128)(2,1)}) %all-gather.5.cloned.1.call-update) | async-done | bytes 2097168 | tf_op jit(solution)/shard_map/all_gather | solution.py:243
  138.7 5.3 %fusion.9 = bf16[1024,1024]{1,0:T(8,128)(2,1)} fusion(bf16[1024,1024]{1,0:T(8,128)(2,1)} %all-gather.5.cloned.1.call-done, bf16[1,1024,1024]{2,1,0:T(8,128)(2,1)S(1)} %copy-done), kind=kOutput, calls=%fused_computation.16 | convolution fusion | flops 2148532224 | bytes 6291456 | tf_op jit(solution)/shard_map/dot_general | solution.py:245
  144.2 2.1 fusion.13
  146.4 23.1 %all-gather.7.cloned.1.call-done = bf16[64,128,128]{2,1,0:T(8,128)(2,1)} async-done(((bf16[8,128,128]{2,1,0:T(8,128)(2,1)}), bf16[64,128,128]{2,1,0:T(8,128)(2,1)}) %all-gather.7.cloned.1.call-update) | async-done | bytes 2097168 | tf_op jit(solution)/shard_map/all_gather | solution.py:27
  169.5 10.7 %while.28 = (s32[]{:T(128)}, f32[8,128,128]{2,1,0:T(8,128)S(1)}, s32[]{:T(128)}, bf16[8,8,128]{2,1,0:T(8,128)(2,1)S(1)}, bf16[8,8,128,128]{3,2,1,0:T(8,128)(2,1)}, /*index=5*/s32[]{:T(128)}, s32[]{:T(128)}) while((s32[]{:T(128)}, f32[8,128,128]{2,1,0:T(8,128)S(1)}, s32[]{:T(128)}, bf16[8,8,128]{2,1,0:T(8,128)(2,1)S(1)}, ...), condition=%wide.region_6.7_spmd.clone, body=%wide.region_5.6_spmd.clone.sunk | while | flops 656388 | bytes 1321065 | solution.py:44
  182.8 4.0 %convolution_convert_fusion = bf16[128,2048]{1,0:T(8,128)(2,1)} fusion(bf16[1024,2048]{1,0:T(8,128)(2,1)} %param.29, bf16[128,1024]{1,0:T(8,128)(2,1)} %param.25, f32[16,8,8,128]{3,2,1,0:T(8,128)S(1)} %bitcast.133, f32[16,8,8,128]{3,2,1,0:T(8,128)S(1)} %bitcast.134, f32[1024]{0:T(1024)S(1)} %copy-done.19), kind=kOutput, calls=%fused_computation.10 | convolution fusion | flops 538312704 | bytes 6033408 | tf_op jit(solution)/shard_map/dot_general | solution.py:121
  188.9 2.1 fusion.15
  191.0 6.3 %all_gather.19 = bf16[128,1024]{1,0:T(8,128)(2,1)S(1)} all-gather(bf16[128,512]{1,0:T(8,128)(2,1)S(1)} %fusion.15), channel_id=1, replica_groups=mesh['grp'=2,'ep'=8,'tp'=2] {'tp'}, dimensions={1}, use_global_device_ids=true | all-gather | bytes 393216 | tf_op jit(solution)/shard_map/all_gather | solution.py:242
  197.3 9.8 %reduce-scatter.5.cloned.1.call-done = bf16[128,1024]{1,0:T(8,128)(2,1)} async-done(((bf16[1024,1024]{1,0:T(8,128)(2,1)}), bf16[128,1024]{1,0:T(8,128)(2,1)}) %reduce-scatter.5.cloned.1.call-update) | async-done | bytes 262160 | tf_op jit(solution)/shard_map/reduce_scatter | solution.py:248
  207.1 2.7 %fusion.14 = bf16[128,1024]{1,0:T(8,128)(2,1)} fusion(bf16[128,1024]{1,0:T(8,128)(2,1)S(1)} %all_gather.19, bf16[1024,1024]{1,0:T(8,128)(2,1)} %param.39, bf16[128,1024]{1,0:T(8,128)(2,1)} %reduce-scatter.5.cloned.1.call-done), kind=kOutput, calls=%fused_computation.24 | convolution fusion | flops 268828672 | bytes 2883584 | tf_op jit(solution)/shard_map/dot_general | solution.py:244
  209.8 13.3 %reduce-scatter.3.cloned.1.call-done = bf16[64,2048]{1,0:T(8,128)(2,1)} async-done(((bf16[128,2048]{1,0:T(8,128)(2,1)}), bf16[64,2048]{1,0:T(8,128)(2,1)}) %reduce-scatter.3.cloned.1.call-update) | async-done | bytes 262160 | tf_op jit(solution)/shard_map/reduce_scatter | solution.py:120
  (131 shorter events, 44.9 us)
Async XLA Ops:
  7.2 131.5 %copy-start = (bf16[1,1024,1024]{2,1,0:T(8,128)(2,1)S(1)}, bf16[1,1024,1024]{2,1,0:T(8,128)(2,1)}, u32[]{:S(2)}) copy-start(bf16[1,1024,1024]{2,1,0:T(8,128)(2,1)} %param.36) | copy-start | bytes 6291460
  7.2 74.6 %copy-start.13 = (bf16[128,1024]{1,0:T(8,128)(2,1)S(1)}, bf16[128,1024]{1,0:T(8,128)(2,1)}, u32[]{:S(2)}) copy-start(bf16[128,1024]{1,0:T(8,128)(2,1)} %param.22) | copy-start | bytes 786436
  7.2 131.5 %all-gather.5.cloned.1.call-start = ((), (), s32[]{:S(2)}) async-start(), calls=%async_computation.3 | async-start | bytes 3145728 | tf_op jit(solution)/shard_map/all_gather | solution.py:243
  12.2 58.5 %copy-start.1 = (bf16[128,2048]{1,0:T(8,128)(2,1)}, bf16[128,2048]{1,0:T(8,128)(2,1)S(1)}, u32[]{:S(2)}) copy-start(bf16[128,2048]{1,0:T(8,128)(2,1)S(1)} %fusion.20) | copy-start | bytes 1572868
  12.5 11.8 %collective-permute-start = (bf16[128,2176]{1,0:T(8,128)(2,1)S(1)}, bf16[128,2176]{1,0:T(8,128)(2,1)S(1)}, u32[]{:S(2)}, u32[]{:S(2)}) collective-permute-start(bf16[128,2176]{1,0:T(8,128)(2,1)S(1)} %concatenate.9), channel_id=1, source_target_pairs={{0,2},{2,4},{4,6},{6,8},{8,10},{10,12},{12,14},{14,0},{1,3},{3,5},... | collective-permute-start | bytes 1671176 | tf_op jit(solution)/shard_map/ppermute | solution.py:18
  25.1 10.8 %collective-permute-start.1 = (bf16[128,2176]{1,0:T(8,128)(2,1)S(1)}, bf16[128,2176]{1,0:T(8,128)(2,1)S(1)}, u32[]{:S(2)}, u32[]{:S(2)}) collective-permute-start(bf16[128,2176]{1,0:T(8,128)(2,1)S(1)} %collective-permute-done), channel_id=1, source_target_pairs={{0,2},{2,4},{4,6},{6,8},{8,10},{10,12},{12,14},{14,0},{1,3},{3,5},... | collective-permute-start | bytes 1671176 | tf_op jit(solution)/shard_map/ppermute | solution.py:18
  36.7 10.8 %collective-permute-start.2 = (bf16[128,2176]{1,0:T(8,128)(2,1)S(1)}, bf16[128,2176]{1,0:T(8,128)(2,1)S(1)}, u32[]{:S(2)}, u32[]{:S(2)}) collective-permute-start(bf16[128,2176]{1,0:T(8,128)(2,1)S(1)} %collective-permute-done.1), channel_id=1, source_target_pairs={{0,2},{2,4},{4,6},{6,8},{8,10},{10,12},{12,14},{14,0},{1,3},{3,5},... | collective-permute-start | bytes 1671176 | tf_op jit(solution)/shard_map/ppermute | solution.py:18
  48.3 10.8 %collective-permute-start.3 = (bf16[128,2176]{1,0:T(8,128)(2,1)S(1)}, bf16[128,2176]{1,0:T(8,128)(2,1)S(1)}, u32[]{:S(2)}, u32[]{:S(2)}) collective-permute-start(bf16[128,2176]{1,0:T(8,128)(2,1)S(1)} %collective-permute-done.2), channel_id=1, source_target_pairs={{0,2},{2,4},{4,6},{6,8},{8,10},{10,12},{12,14},{14,0},{1,3},{3,5},... | collective-permute-start | bytes 1671176 | tf_op jit(solution)/shard_map/ppermute | solution.py:18
  59.8 10.9 %collective-permute-start.4 = (bf16[128,2176]{1,0:T(8,128)(2,1)S(1)}, bf16[128,2176]{1,0:T(8,128)(2,1)}, u32[]{:S(2)}, u32[]{:S(2)}) collective-permute-start(bf16[128,2176]{1,0:T(8,128)(2,1)S(1)} %collective-permute-done.3), channel_id=1, source_target_pairs={{0,2},{2,4},{4,6},{6,8},{8,10},{10,12},{12,14},{14,0},{1,3},{3,5},... | collective-permute-start | bytes 1671176 | tf_op jit(solution)/shard_map/ppermute | solution.py:18
  70.7 11.1 %collective-permute-start.5 = (bf16[128,2176]{1,0:T(8,128)(2,1)}, bf16[128,2176]{1,0:T(8,128)(2,1)}, u32[]{:S(2)}, u32[]{:S(2)}) collective-permute-start(bf16[128,2176]{1,0:T(8,128)(2,1)} %collective-permute-done.4), channel_id=1, source_target_pairs={{0,2},{2,4},{4,6},{6,8},{8,10},{10,12},{12,14},{14,0},{1,3},{3,5},... | collective-permute-start | bytes 1671176 | tf_op jit(solution)/shard_map/ppermute | solution.py:18
  71.5 11.3 %copy-start.16 = (bf16[128,1024]{1,0:T(8,128)(2,1)S(1)}, bf16[128,1024]{1,0:T(8,128)(2,1)}, u32[]{:S(2)}) copy-start(bf16[128,1024]{1,0:T(8,128)(2,1)} %param.24) | copy-start | bytes 786436
  81.8 11.1 %collective-permute-start.6 = (bf16[128,2176]{1,0:T(8,128)(2,1)}, bf16[128,2176]{1,0:T(8,128)(2,1)}, u32[]{:S(2)}, u32[]{:S(2)}) collective-permute-start(bf16[128,2176]{1,0:T(8,128)(2,1)} %collective-permute-done.5), channel_id=1, source_target_pairs={{0,2},{2,4},{4,6},{6,8},{8,10},{10,12},{12,14},{14,0},{1,3},{3,5},... | collective-permute-start | bytes 1671176 | tf_op jit(solution)/shard_map/ppermute | solution.py:18
  82.9 13.3 %copy-start.11 = (bf16[128,2176]{1,0:T(8,128)(2,1)S(1)}, bf16[128,2176]{1,0:T(8,128)(2,1)}, u32[]{:S(2)}) copy-start(bf16[128,2176]{1,0:T(8,128)(2,1)} %copy-done.10) | copy-start | bytes 1671172
  82.9 13.3 %copy-start.9 = (bf16[128,2176]{1,0:T(8,128)(2,1)S(1)}, bf16[128,2176]{1,0:T(8,128)(2,1)}, u32[]{:S(2)}) copy-start(bf16[128,2176]{1,0:T(8,128)(2,1)} %copy-done.8) | copy-start | bytes 1671172
  82.9 13.4 %copy-start.7 = (bf16[128,2176]{1,0:T(8,128)(2,1)S(1)}, bf16[128,2176]{1,0:T(8,128)(2,1)}, u32[]{:S(2)}) copy-start(bf16[128,2176]{1,0:T(8,128)(2,1)} %copy-done.6) | copy-start | bytes 1671172
  82.9 13.5 %copy-start.5 = (bf16[128,2176]{1,0:T(8,128)(2,1)S(1)}, bf16[128,2176]{1,0:T(8,128)(2,1)}, u32[]{:S(2)}) copy-start(bf16[128,2176]{1,0:T(8,128)(2,1)} %copy-done.4) | copy-start | bytes 1671172
  106.7 62.7 %all-gather.7.cloned.1.call-start = ((), (), s32[]{:S(2)}) async-start(), calls=%async_computation.5 | async-start | bytes 2359296 | tf_op jit(solution)/shard_map/all_gather | solution.py:27
  115.8 91.3 %reduce-scatter.5.cloned.1.call-start = ((), (), s32[]{:S(2)}) async-start(), calls=%async_computation.4 | async-start | bytes 2359296 | tf_op jit(solution)/shard_map/reduce_scatter | solution.py:248
  129.4 14.8 %copy-start.14 = (bf16[8,2,64,128]{3,0,1,2:T(8,128)(2,1)S(1)}, bf16[8,2,64,128]{3,0,1,2:T(8,128)(2,1)}, u32[]{:S(2)}) copy-start(bf16[8,2,64,128]{3,0,1,2:T(8,128)(2,1)} %get-tuple-element.188) | copy-start | bytes 786436
  129.4 14.8 %copy-start.15 = (bf16[8,2,64,128]{3,0,1,2:T(8,128)(2,1)S(1)}, bf16[8,2,64,128]{3,0,1,2:T(8,128)(2,1)}, u32[]{:S(2)}) copy-start(bf16[8,2,64,128]{3,0,1,2:T(8,128)(2,1)} %get-tuple-element.189) | copy-start | bytes 786436
  144.0 36.2 %copy-start.12 = (bf16[8,2,64,128]{3,0,1,2:T(8,128)(2,1)S(1)}, bf16[8,2,64,128]{3,0,1,2:T(8,128)(2,1)}, u32[]{:S(2)}) copy-start(bf16[8,2,64,128]{3,0,1,2:T(8,128)(2,1)} %get-tuple-element.190) | copy-start | bytes 786436
  144.0 79.2 %reduce-scatter.3.cloned.1.call-start = ((), (), s32[]{:S(2)}) async-start(), calls=%async_computation.2 | async-start | bytes 786432 | tf_op jit(solution)/shard_map/reduce_scatter | solution.py:120
  169.5 13.3 %copy-start.19 = (f32[1024]{0:T(1024)S(1)}, f32[1024]{0:T(1024)}, u32[]{:S(2)}) copy-start(f32[1024]{0:T(1024)} %param.28) | copy-start | bytes 12292
  182.6 4.3 %copy-start.2 = (bf16[128,2048]{1,0:T(8,128)(2,1)S(1)}, bf16[128,2048]{1,0:T(8,128)(2,1)}, u32[]{:S(2)}) copy-start(bf16[128,2048]{1,0:T(8,128)(2,1)} %copy-done.1) | copy-start | bytes 1572868
  (7 other events, 13.5 us)
Sparse Core Ops, SparseCore 0:
  106.9 31.7 all-gather.4
  140.3 29.1 all-gather.6
  171.8 35.2 reduce-scatter.4
  209.7 13.3 reduce-scatter.2
